TPU v7x, 256 devices: a whole 4x4x8 slice. The times are simulated.
256 devices in a mesh: sp: 32 (over z, y), tp: 8 (over x, core).
Axes of the slice: x: 4, y: 4, z: 8, core: 2. Of those that a mesh axis runs over, the one named last changes fastest.
Arguments:
- queries: bfloat16 [16384, 1024], P('sp', 'tp'), may hold values from -200 to 200
- keys: bfloat16 [16384, 1024], P('sp', 'tp'), may hold values from -6 to 6
- values: bfloat16 [16384, 1024], P('sp', 'tp'), may hold values from -24 to 24
- cum_gate: float32 [16384, 8], P('sp', 'tp'), may hold values from -1643 to 0, as said below
- residual: bfloat16 [16384, 2048], P(('sp', 'tp')), may hold values from -1.5 to 1.5
- w_out: bfloat16 [1024, 2048], replicated, may hold values from -0.1875 to 0.1875
- gain: float32 [2048], replicated, may hold values from 0.1 to 1.9
- w_up: bfloat16 [2048, 8192], P('sp', 'tp'), may hold values from -0.125 to 0.125
- w_down: bfloat16 [8192, 2048], P('tp', 'sp'), may hold values from -0.0625 to 0.0625
Outputs:
- output: bfloat16 [16384, 2048], P(('sp', 'tp'))
Inputs may be any that keep to these rules, and one draw needn't show every extreme that they name: Within each head, cum_gate never rises from one position to the next.
All inputs are finite; a program needn't handle non-finite values.
Results may differ from a plain program's by a relative error of at most 0.022.
Values may be sent and summed in bfloat16 or wider, within the bound.
A program may use at most 128 MiB of HBM per device.

v0:
```python
import math

import jax
import jax.numpy as jnp
from jax import lax
from jax.sharding import Mesh
from jax.sharding import PartitionSpec as P

SP = ("sp_0", "sp_1")
SP_TP = ("sp_0", "sp_1", "tp")


def joined_along(tiles, dim):
    dims = list(tiles.shape[1:])
    dims[dim] *= tiles.shape[0]
    return jnp.moveaxis(tiles, 0, dim).reshape(dims)


def copy_for_each(shard, axis):
    devices = lax.axis_size(axis)
    return lax.all_to_all(
        jnp.broadcast_to(shard[None], (devices, *shard.shape)), axis, 0, 0, tiled=True
    )


def collect(shard, axis, dim):
    return joined_along(copy_for_each(shard, axis), dim)


def sent_together(arrays, axis, dim, along):
    widths = [a.shape[along] for a in arrays]
    both = jnp.concatenate(arrays, axis=along)
    filled = lax.all_gather(both, axis, axis=dim, tiled=True)
    return tuple(jnp.split(filled, [sum(widths[:k]) for k in range(1, len(widths))], axis=along))


def whole_of(shard, axes, dim):
    filled = shard
    for number in range(len(axes) - 1, -1, -1):
        filled = lax.all_gather(filled, axes[number], axis=dim, tiled=True)
    return filled


def in_blocks(shard, dim, devices):
    before, after = (shard.shape[:dim], shard.shape[dim + 1 :])
    return jnp.moveaxis(shard.reshape(*before, devices, -1, *after), dim, 0)


def sum_at_owner(shard, axis, dim):
    tiles = in_blocks(shard, dim, lax.axis_size(axis))
    arrived = lax.all_to_all(tiles, axis, split_axis=0, concat_axis=0, tiled=True)
    return arrived.astype(jnp.float32).sum(axis=0)


def per_device(queries, keys, values, cum_gate, residual, w_out, gain, w_up, w_down):
    tok_rows, width = queries.shape
    heads_here = cum_gate.shape[1]
    head_size = width // heads_here
    score_scale = head_size ** (-0.5)
    row_offset = lax.axis_index(SP) * tok_rows
    query_heads = queries.reshape(tok_rows, heads_here, head_size)
    query_pos = row_offset + jnp.arange(tok_rows, dtype=jnp.int32)
    all_gates = collect(cum_gate, SP, 0)
    initial = (
        jnp.full((tok_rows, heads_here), -1e30, jnp.float32),
        jnp.zeros((tok_rows, heads_here), jnp.float32),
        jnp.zeros((tok_rows, heads_here, head_size), jnp.float32),
    )
    carried = initial
    key_rows, value_rows = sent_together((keys, values), SP, 0, 1)
    row_count = key_rows.shape[0]
    span_rows = math.gcd(row_count, 2048)
    block_count = row_count // span_rows
    key_blocks = key_rows.reshape(block_count, span_rows, heads_here, head_size)
    value_blocks = value_rows.reshape(block_count, span_rows, heads_here, head_size)
    first_pos = jnp.arange(block_count, dtype=jnp.int32) * span_rows

    def absorb_block(running, packed):
        running_max, running_sum, accumulated = running
        key_blk, value_blk, block_start = packed
        gate_blk = lax.dynamic_slice_in_dim(all_gates, block_start, span_rows, 0)
        scores = jnp.einsum(
            "qhd,khd->qhk", query_heads, key_blk, preferred_element_type=jnp.float32
        )
        scores = scores * score_scale + cum_gate[:, :, None] - gate_blk.T[None, :, :]
        key_pos = block_start + jnp.arange(span_rows, dtype=jnp.int32)
        scores = jnp.where(key_pos[None, None, :] <= query_pos[:, None, None], scores, -1e30)
        new_max = jnp.maximum(running_max, jnp.max(scores, axis=-1))
        rescale = jnp.exp(running_max - new_max)
        weights = jnp.exp(scores - new_max[:, :, None])
        running_sum = running_sum * rescale + jnp.sum(weights, axis=-1)
        product = jnp.einsum(
            "qhk,khd->qhd",
            weights.astype(jnp.bfloat16),
            value_blk,
            preferred_element_type=jnp.float32,
        )
        accumulated = accumulated * rescale[:, :, None] + product
        return ((new_max, running_sum, accumulated), None)

    carried, _ = lax.scan(absorb_block, carried, (key_blocks, value_blocks, first_pos))
    running_max, running_sum, accumulated = carried
    attended = (accumulated / running_sum[:, :, None]).reshape(tok_rows, width).astype(jnp.bfloat16)
    mine = lax.all_to_all(attended, "tp", split_axis=0, concat_axis=1, tiled=True)
    projected = jnp.dot(mine, w_out, preferred_element_type=jnp.float32)
    residual_sum = residual.astype(jnp.float32) + projected
    mean_square = jnp.mean(residual_sum * residual_sum, axis=-1, keepdims=True)
    normed = (residual_sum * lax.rsqrt(mean_square + 1e-06) * gain).astype(jnp.bfloat16)
    normed_all = collect(normed, "tp", 0)
    up_proj = jnp.dot(normed_all, whole_of(w_up, SP, 0), preferred_element_type=jnp.float32)
    hidden = jnp.square(jax.nn.relu(up_proj)).astype(jnp.bfloat16)
    down_whole = whole_of(w_down, SP, 1)
    rounded = jnp.dot(hidden, down_whole, preferred_element_type=jnp.float32).astype(jnp.bfloat16)
    branch_out = sum_at_owner(
        lax.optimization_barrier(rounded).astype(jnp.float32).astype(jnp.bfloat16), "tp", 0
    )
    return (residual_sum + branch_out).astype(jnp.bfloat16)


def solution(mesh):
    finer = Mesh(mesh.devices.reshape(8, 4, mesh.shape["tp"]), ("sp_0", "sp_1", "tp"))
    in_specs = (
        P(SP, "tp"),
        P(SP, "tp"),
        P(SP, "tp"),
        P(SP, "tp"),
        P(SP_TP, None),
        P(),
        P(),
        P(SP, "tp"),
        P("tp", SP),
    )
    out_specs = P(SP_TP, None)
    return jax.shard_map(
        per_device, mesh=finer, in_specs=in_specs, out_specs=out_specs, check_vma=False
    )
```

profile of v0, /device:TPU:1, one launch (start us, length us, event | category | flops | bytes accessed | tf_op | source)
XLA Modules:
  0.0 313.7 jit_solution(8146533868833869425)
XLA Ops:
  6.5 1.7 pad_maximum_fusion
  8.3 13.3 %all_gather.16 = bf16[256,1024]{1,0:T(8,128)(2,1)} all-gather(bf16[64,1024]{1,0:T(8,128)(2,1)} %param.18), channel_id=1, replica_groups=mesh['sp_0'=8,'sp_1'=4,'tp'=8] {'sp_1'}, dimensions={0}, use_global_device_ids=true | all-gather | bytes 655360 | tf_op jit(solution)/shard_map/all_gather | solution.py:40
  21.6 1.3 broadcast_in_dim.25
  23.0 9.5 %all-to-all-start = ((f32[32,512,1]{1,2,0:T(1,128)}), f32[32,512,1]{1,2,0:T(1,128)S(1)}, u32[]{:S(2)}, u32[]{:S(2)}) async-start(f32[32,512,1]{1,2,0:T(1,128)} %broadcast_in_dim.25), calls=%async_computation | async-start | bytes 131072 | tf_op jit(solution)/shard_map/all_to_all | solution.py:21
  32.5 12.9 %all_gather.18 = bf16[1024,256]{0,1:T(8,128)(2,1)} all-gather(bf16[1024,64]{0,1:T(8,128)(2,1)} %param.19), channel_id=1, replica_groups=mesh['sp_0'=8,'sp_1'=4,'tp'=8] {'sp_1'}, dimensions={1}, use_global_device_ids=true | all-gather | bytes 655360 | tf_op jit(solution)/shard_map/all_gather | solution.py:40
  45.5 65.7 %all-gather.4.cloned.1.call-done = bf16[16384,256]{1,0:T(8,128)(2,1)} async-done(((bf16[512,256]{1,0:T(8,128)(2,1)}), bf16[16384,256]{1,0:T(8,128)(2,1)}) %all-gather.4.cloned.1.call-update) | async-done | bytes 8388624 | tf_op jit(solution)/shard_map/all_gather | solution.py:33
  111.3 5.7 %fusion.29 = (bf16[16384,128]{1,0:T(8,128)(2,1)}, bf16[16384,128]{1,0:T(8,128)(2,1)}) fusion(bf16[16384,256]{1,0:T(8,128)(2,1)} %all-gather.4.cloned.1.call-done), kind=kLoop, calls=%fused_computation.44 | loop fusion | bytes 16777216 | tf_op jit(solution)/shard_map/split | solution.py:34
  117.0 102.6 %while.15 = (s32[]{:T(128)}, f32[512,1]{0,1:T(1,128)S(1)}, f32[512,1]{0,1:T(1,128)S(1)}, f32[512,1,128]{0,2,1:T(8,128)S(1)}, s32[8]{0:T(128)S(1)}, /*index=5*/bf...) while((s32[]{:T(128)}, f32[512,1]{0,1:T(1,128)S(1)}, ...), condition=%wide.region_3.4_spmd.clone, body=%wide.region_0.3_spmd.clone.sunk | while | flops 547558400 | bytes 31145188 | solution.py:101
  117.0 0.6 dynamic_slice.36
  119.6 0.7 iota_add_fusion.5
  120.3 4.0 %fusion.44 = (f32[512]{0:T(512)S(1)}, f32[512,1,2048]{0,2,1:T(8,128)}) fusion(f32[2048]{0:T(1024)S(1)} %bitcast.101, f32[512]{0:T(512)S(1)} %bitcast.106, bf16[512,1,128]{2,0,1:T(8,128)(2,1)S(1)} %get-tuple-element.265, bf16[8,2048,1,128]{3,1,2,0:T(8,128)(2,1)} %get-tuple-element.264, s32[]{:T(128)} %get-tuple-element.245, ...), kind=kOutput, calls=%fused_computation.43.clone.1 | convolution fusion | flops 274726400 | bytes 4872704 | tf_op jit(solution)/shard_map/while/body/eval_jaxpr/qhd,khd->qhk/dot_general | solution.py:82
  124.4 3.0 fusion.46
  127.4 0.4 copy-done
  127.8 2.0 fusion.48
  129.8 0.6 dynamic_slice.36
  132.4 0.7 iota_add_fusion.5
  133.1 4.0 %fusion.44 = (f32[512]{0:T(512)S(1)}, f32[512,1,2048]{0,2,1:T(8,128)}) fusion(f32[2048]{0:T(1024)S(1)} %bitcast.101, f32[512]{0:T(512)S(1)} %bitcast.106, bf16[512,1,128]{2,0,1:T(8,128)(2,1)S(1)} %get-tuple-element.265, bf16[8,2048,1,128]{3,1,2,0:T(8,128)(2,1)} %get-tuple-element.264, s32[]{:T(128)} %get-tuple-element.245, ...), kind=kOutput, calls=%fused_computation.43.clone.1 | convolution fusion | flops 274726400 | bytes 4872704 | tf_op jit(solution)/shard_map/while/body/eval_jaxpr/qhd,khd->qhk/dot_general | solution.py:82
  137.1 3.0 fusion.46
  140.2 0.5 copy-done
  140.7 1.9 fusion.48
  142.6 0.6 dynamic_slice.36
  145.3 0.7 iota_add_fusion.5
  145.9 4.0 %fusion.44 = (f32[512]{0:T(512)S(1)}, f32[512,1,2048]{0,2,1:T(8,128)}) fusion(f32[2048]{0:T(1024)S(1)} %bitcast.101, f32[512]{0:T(512)S(1)} %bitcast.106, bf16[512,1,128]{2,0,1:T(8,128)(2,1)S(1)} %get-tuple-element.265, bf16[8,2048,1,128]{3,1,2,0:T(8,128)(2,1)} %get-tuple-element.264, s32[]{:T(128)} %get-tuple-element.245, ...), kind=kOutput, calls=%fused_computation.43.clone.1 | convolution fusion | flops 274726400 | bytes 4872704 | tf_op jit(solution)/shard_map/while/body/eval_jaxpr/qhd,khd->qhk/dot_general | solution.py:82
  150.0 3.0 fusion.46
  153.0 0.5 copy-done
  153.5 1.9 fusion.48
  155.5 0.6 dynamic_slice.36
  158.1 0.7 iota_add_fusion.5
  158.8 4.0 %fusion.44 = (f32[512]{0:T(512)S(1)}, f32[512,1,2048]{0,2,1:T(8,128)}) fusion(f32[2048]{0:T(1024)S(1)} %bitcast.101, f32[512]{0:T(512)S(1)} %bitcast.106, bf16[512,1,128]{2,0,1:T(8,128)(2,1)S(1)} %get-tuple-element.265, bf16[8,2048,1,128]{3,1,2,0:T(8,128)(2,1)} %get-tuple-element.264, s32[]{:T(128)} %get-tuple-element.245, ...), kind=kOutput, calls=%fused_computation.43.clone.1 | convolution fusion | flops 274726400 | bytes 4872704 | tf_op jit(solution)/shard_map/while/body/eval_jaxpr/qhd,khd->qhk/dot_general | solution.py:82
  162.8 3.0 fusion.46
  165.8 0.4 copy-done
  166.3 1.9 fusion.48
  168.3 0.6 dynamic_slice.36
  170.9 0.7 iota_add_fusion.5
  171.5 4.0 %fusion.44 = (f32[512]{0:T(512)S(1)}, f32[512,1,2048]{0,2,1:T(8,128)}) fusion(f32[2048]{0:T(1024)S(1)} %bitcast.101, f32[512]{0:T(512)S(1)} %bitcast.106, bf16[512,1,128]{2,0,1:T(8,128)(2,1)S(1)} %get-tuple-element.265, bf16[8,2048,1,128]{3,1,2,0:T(8,128)(2,1)} %get-tuple-element.264, s32[]{:T(128)} %get-tuple-element.245, ...), kind=kOutput, calls=%fused_computation.43.clone.1 | convolution fusion | flops 274726400 | bytes 4872704 | tf_op jit(solution)/shard_map/while/body/eval_jaxpr/qhd,khd->qhk/dot_general | solution.py:82
  175.6 3.1 fusion.46
  178.7 0.5 copy-done
  179.2 1.9 fusion.48
  181.2 0.6 dynamic_slice.36
  183.8 0.7 iota_add_fusion.5
  184.5 4.0 %fusion.44 = (f32[512]{0:T(512)S(1)}, f32[512,1,2048]{0,2,1:T(8,128)}) fusion(f32[2048]{0:T(1024)S(1)} %bitcast.101, f32[512]{0:T(512)S(1)} %bitcast.106, bf16[512,1,128]{2,0,1:T(8,128)(2,1)S(1)} %get-tuple-element.265, bf16[8,2048,1,128]{3,1,2,0:T(8,128)(2,1)} %get-tuple-element.264, s32[]{:T(128)} %get-tuple-element.245, ...), kind=kOutput, calls=%fused_computation.43.clone.1 | convolution fusion | flops 274726400 | bytes 4872704 | tf_op jit(solution)/shard_map/while/body/eval_jaxpr/qhd,khd->qhk/dot_general | solution.py:82
  188.5 3.0 fusion.46
  191.6 0.5 copy-done
  192.1 1.9 fusion.48
  194.0 0.6 dynamic_slice.36
  196.6 0.7 iota_add_fusion.5
  197.3 4.0 %fusion.44 = (f32[512]{0:T(512)S(1)}, f32[512,1,2048]{0,2,1:T(8,128)}) fusion(f32[2048]{0:T(1024)S(1)} %bitcast.101, f32[512]{0:T(512)S(1)} %bitcast.106, bf16[512,1,128]{2,0,1:T(8,128)(2,1)S(1)} %get-tuple-element.265, bf16[8,2048,1,128]{3,1,2,0:T(8,128)(2,1)} %get-tuple-element.264, s32[]{:T(128)} %get-tuple-element.245, ...), kind=kOutput, calls=%fused_computation.43.clone.1 | convolution fusion | flops 274726400 | bytes 4872704 | tf_op jit(solution)/shard_map/while/body/eval_jaxpr/qhd,khd->qhk/dot_general | solution.py:82
  201.4 3.0 fusion.46
  204.4 0.5 copy-done
  204.9 1.9 fusion.48
  206.9 0.6 dynamic_slice.36
  209.5 0.7 iota_add_fusion.5
  210.1 4.0 %fusion.44 = (f32[512]{0:T(512)S(1)}, f32[512,1,2048]{0,2,1:T(8,128)}) fusion(f32[2048]{0:T(1024)S(1)} %bitcast.101, f32[512]{0:T(512)S(1)} %bitcast.106, bf16[512,1,128]{2,0,1:T(8,128)(2,1)S(1)} %get-tuple-element.265, bf16[8,2048,1,128]{3,1,2,0:T(8,128)(2,1)} %get-tuple-element.264, s32[]{:T(128)} %get-tuple-element.245, ...), kind=kOutput, calls=%fused_computation.43.clone.1 | convolution fusion | flops 274726400 | bytes 4872704 | tf_op jit(solution)/shard_map/while/body/eval_jaxpr/qhd,khd->qhk/dot_general | solution.py:82
  214.2 3.0 fusion.46
  217.2 0.4 copy-done
  217.7 1.9 fusion.48
  219.9 10.7 %all_to_all.31 = bf16[8,64,128]{2,1,0:T(8,128)(2,1)S(1)} all-to-all(bf16[8,64,128]{2,1,0:T(8,128)(2,1)S(1)} %bitcast.98), channel_id=1, replica_groups=mesh['sp_0'=8,'sp_1'=4,'tp'=8] {'tp'}, dimensions={0} | all-to-all | bytes 262144 | tf_op jit(solution)/shard_map/all_to_all | solution.py:104
  230.6 3.2 %multiply_reduce_fusion = (f32[64]{0:T(128)S(1)}, f32[64,2048]{1,0:T(8,128)S(1)}) fusion(bf16[1024,2048]{1,0:T(8,128)(2,1)} %param.16, bf16[64,2048]{1,0:T(8,128)(2,1)S(1)} %copy-done.1, bf16[8,64,128]{2,1,0:T(8,128)(2,1)S(1)} %all_to_all.31), kind=kOutput, calls=%fused_computation.35 | convolution fusion | flops 268959680 | bytes 5112064 | tf_op jit(solution)/shard_map/dot_general | solution.py:105
  233.9 1.6 broadcast_in_dim.40
  235.5 4.4 %all-to-all-start.2 = ((bf16[8,64,2048]{2,1,0:T(8,128)(2,1)}), bf16[8,64,2048]{2,1,0:T(8,128)(2,1)S(1)}, u32[]{:S(2)}, u32[]{:S(2)}) async-start(bf16[8,64,2048]{2,1,0:T(8,128)(2,1)} %broadcast_in_dim.40), calls=%async_computation.2 | async-start | bytes 4194304 | tf_op jit(solution)/shard_map/all_to_all | solution.py:21
  239.9 26.2 %all-to-all-done.2 = bf16[8,64,2048]{2,1,0:T(8,128)(2,1)S(1)} async-done(((bf16[8,64,2048]{2,1,0:T(8,128)(2,1)}), bf16[8,64,2048]{2,1,0:T(8,128)(2,1)S(1)}, u32[]{:S(2)}, u32[]{:S(2)}) %all-to-all-start.2) | async-done | bytes 2097184 | tf_op jit(solution)/shard_map/all_to_all | solution.py:21
  266.1 9.3 %convolution_convert_fusion = bf16[512,2048]{1,0:T(8,128)(2,1)} fusion(bf16[1024,2048]{0,1:T(8,128)(2,1)} %all-gather.8.cloned.1.call-done, bf16[512,2048]{1,0:T(8,128)(2,1)S(1)} %bitcast.94, bf16[2048,1024]{1,0:T(8,128)(2,1)} %all-gather.6.cloned.1.call-done), kind=kOutput, calls=%fused_computation.30 | convolution fusion | flops 4297588736 | bytes 12582912 | tf_op jit(solution)/shard_map/dot_general | solution.py:113
  275.4 30.6 %all_to_all.32 = bf16[8,64,2048]{2,1,0:T(8,128)(2,1)S(1)} all-to-all(bf16[8,64,2048]{2,1,0:T(8,128)(2,1)} %bitcast.95), channel_id=1, replica_groups=mesh['sp_0'=8,'sp_1'=4,'tp'=8] {'tp'}, dimensions={0} | all-to-all | bytes 4194304 | tf_op jit(solution)/shard_map/all_to_all | solution.py:51
  306.4 0.8 add_convert_fusion
  (74 shorter events, 1.9 us)
Async XLA Ops:
  6.5 104.7 %all-gather.4.cloned.1.call-start = ((), (), s32[]{:S(2)}) async-start(), calls=%async_computation.4 | async-start | bytes 8650752 | tf_op jit(solution)/shard_map/all_gather | solution.py:33
  8.3 231.6 %all-gather.6.cloned.1.call-start = ((), (), s32[]{:S(2)}) async-start(), calls=%async_computation.5 | async-start | bytes 4718592 | tf_op jit(solution)/shard_map/all_gather | solution.py:40
  23.0 94.0 %all-to-all-start = ((f32[32,512,1]{1,2,0:T(1,128)}), f32[32,512,1]{1,2,0:T(1,128)S(1)}, u32[]{:S(2)}, u32[]{:S(2)}) async-start(f32[32,512,1]{1,2,0:T(1,128)} %broadcast_in_dim.25), calls=%async_computation | async-start | bytes 131072 | tf_op jit(solution)/shard_map/all_to_all | solution.py:21
  32.4 207.4 %all-gather.8.cloned.1.call-start = ((), (), s32[]{:S(2)}) async-start(), calls=%async_computation.6 | async-start | bytes 4718592 | tf_op jit(solution)/shard_map/all_gather | solution.py:40
  45.5 71.5 %copy-start.3 = (f32[512,1]{0,1:T(1,128)S(1)}, f32[512,1]{0,1:T(1,128)}, u32[]{:S(2)}) copy-start(f32[512,1]{0,1:T(1,128)} %param.14) | copy-start | bytes 6148
  45.5 71.5 %copy-start.4 = (bf16[512,128]{1,0:T(8,128)(2,1)S(1)}, bf16[512,128]{1,0:T(8,128)(2,1)}, u32[]{:S(2)}) copy-start(bf16[512,128]{1,0:T(8,128)(2,1)} %param.11) | copy-start | bytes 393220
  117.0 113.6 %copy-start.1 = (bf16[64,2048]{1,0:T(8,128)(2,1)S(1)}, bf16[64,2048]{1,0:T(8,128)(2,1)}, u32[]{:S(2)}) copy-start(bf16[64,2048]{1,0:T(8,128)(2,1)} %param.15) | copy-start | bytes 786436
  124.4 3.4 %copy-start = (f32[512,1,2048]{0,2,1:T(8,128)S(1)}, f32[512,1,2048]{0,2,1:T(8,128)}, u32[]{:S(2)}) copy-start(f32[512,1,2048]{0,2,1:T(8,128)} %get-tuple-element.228) | copy-start | bytes 12582916 | tf_op jit(solution)/shard_map/while
  137.1 3.5 %copy-start = (f32[512,1,2048]{0,2,1:T(8,128)S(1)}, f32[512,1,2048]{0,2,1:T(8,128)}, u32[]{:S(2)}) copy-start(f32[512,1,2048]{0,2,1:T(8,128)} %get-tuple-element.228) | copy-start | bytes 12582916 | tf_op jit(solution)/shard_map/while
  150.0 3.5 %copy-start = (f32[512,1,2048]{0,2,1:T(8,128)S(1)}, f32[512,1,2048]{0,2,1:T(8,128)}, u32[]{:S(2)}) copy-start(f32[512,1,2048]{0,2,1:T(8,128)} %get-tuple-element.228) | copy-start | bytes 12582916 | tf_op jit(solution)/shard_map/while
  162.8 3.4 %copy-start = (f32[512,1,2048]{0,2,1:T(8,128)S(1)}, f32[512,1,2048]{0,2,1:T(8,128)}, u32[]{:S(2)}) copy-start(f32[512,1,2048]{0,2,1:T(8,128)} %get-tuple-element.228) | copy-start | bytes 12582916 | tf_op jit(solution)/shard_map/while
  175.6 3.6 %copy-start = (f32[512,1,2048]{0,2,1:T(8,128)S(1)}, f32[512,1,2048]{0,2,1:T(8,128)}, u32[]{:S(2)}) copy-start(f32[512,1,2048]{0,2,1:T(8,128)} %get-tuple-element.228) | copy-start | bytes 12582916 | tf_op jit(solution)/shard_map/while
  188.5 3.5 %copy-start = (f32[512,1,2048]{0,2,1:T(8,128)S(1)}, f32[512,1,2048]{0,2,1:T(8,128)}, u32[]{:S(2)}) copy-start(f32[512,1,2048]{0,2,1:T(8,128)} %get-tuple-element.228) | copy-start | bytes 12582916 | tf_op jit(solution)/shard_map/while
  201.4 3.5 %copy-start = (f32[512,1,2048]{0,2,1:T(8,128)S(1)}, f32[512,1,2048]{0,2,1:T(8,128)}, u32[]{:S(2)}) copy-start(f32[512,1,2048]{0,2,1:T(8,128)} %get-tuple-element.228) | copy-start | bytes 12582916 | tf_op jit(solution)/shard_map/while
  214.2 3.5 %copy-start = (f32[512,1,2048]{0,2,1:T(8,128)S(1)}, f32[512,1,2048]{0,2,1:T(8,128)}, u32[]{:S(2)}) copy-start(f32[512,1,2048]{0,2,1:T(8,128)} %get-tuple-element.228) | copy-start | bytes 12582916 | tf_op jit(solution)/shard_map/while
  219.6 14.1 %copy-start.2 = (f32[2048]{0:T(1024)S(1)}, f32[2048]{0:T(1024)}, u32[]{:S(2)}) copy-start(f32[2048]{0:T(1024)} %param.17) | copy-start | bytes 24580
  235.5 30.6 %all-to-all-start.2 = ((bf16[8,64,2048]{2,1,0:T(8,128)(2,1)}), bf16[8,64,2048]{2,1,0:T(8,128)(2,1)S(1)}, u32[]{:S(2)}, u32[]{:S(2)}) async-start(bf16[8,64,2048]{2,1,0:T(8,128)(2,1)} %broadcast_in_dim.40), calls=%async_computation.2 | async-start | bytes 4194304 | tf_op jit(solution)/shard_map/all_to_all | solution.py:21
Sparse Core Ops, SparseCore 0:
  9.9 101.3 all-gather.3
  113.0 52.3 all-gather.5
  167.3 53.3 all-gather.7
where the time goes:
time: 315 us; the launch traced here: 314 us
  waiting for transfers between devices  92 us (29%)
  blocking collectives  67.5 us (21%)
  matrix products  60.3 us (19%)
  other arithmetic  32.6 us (10%)
  local copies, waits for them, and re-layouts  18 us (6%)
  loops' own time  16 us (5%)
  starting transfers between devices  13.9 us (4%)
  between operations  13.3 us (4%)
    all_gather x1, waiting for transfers between devices, sent_together(): filled = lax.all_gather(both, axis, axis=dim, tiled=True)  65.7 us
    dot_general x8, matrix products, absorb_block(): jnp.einsum('qhd,khd->qhk', query_heads, key_blk, preferred_element_type=j...  32.3 us
    all_to_all x1, blocking collectives, sum_at_owner(): lax.all_to_all(tiles, axis, split_axis=0, concat_axis=0, tiled=True)  30.6 us
    all_to_all x2, waiting for transfers between devices, copy_for_each(): lax.all_to_all(jnp.broadcast_to(shard[None], (devices, *shard.shape)), ax...  26.2 us
    all_gather x2, blocking collectives, whole_of(): filled = lax.all_gather(filled, axes[number], axis=dim, tiled=True)  26.2 us
    reduce_sum x8, other arithmetic, absorb_block(): running_sum = running_sum * rescale + jnp.sum(weights, axis=-1)  24.1 us
    another operation x1, loops' own time, per_device(): lax.scan(absorb_block, carried, (key_blocks, value_blocks, first_pos))  16 us
    dot_general x8, matrix products, absorb_block(): jnp.einsum('qhk,khd->qhd', weights.astype(jnp.bfloat16), value_blk, prefe...  15.5 us
  transfers between devices with their start and end apart: 5, of which 2 were waited for; matrix products, arithmetic and copies ran while one was open for 30% of the time, Pallas kernels for 0%

commit v1 on v0

v1 whole, which is shorter than its diff:
```python
import functools
import math

import jax
import jax.numpy as jnp
from jax import lax
from jax.experimental import pallas as pl
from jax.experimental.pallas import tpu as pltpu
from jax.sharding import Mesh
from jax.sharding import PartitionSpec as P

MESH = pl.DeviceIdType.MESH
GRID = (8, 4, 4, 2)
ROW_TILE = 256
COL_TILE = 256
GROUPS = 4
LOW = -1e30


def remote(src, dst, send_sem, recv_sem, device):
    return pltpu.make_async_remote_copy(
        src_ref=src,
        dst_ref=dst,
        send_sem=send_sem,
        recv_sem=recv_sem,
        device_id=device,
        device_id_type=MESH,
    )


def dot(a, b, contract=((1,), (0,))):
    return lax.dot_general(a, b, (contract, ((), ())), preferred_element_type=jnp.float32)


def layer_kernel(
    sizes,
    q_hbm,
    k_hbm,
    v_hbm,
    gate_hbm,
    res_hbm,
    wo_hbm,
    gain_ref,
    up_hbm,
    dn_hbm,
    out_ref,
    q_all,
    kv_all,
    gate_all,
    v_ones,
    top_s,
    acc_s,
    o_send,
    o_recv,
    lse_send,
    lse_recv,
    heads,
    res_all,
    wo_s,
    rsum,
    normed,
    up_all,
    dn_all,
    hidden,
    part,
    pair_recv,
    sum_send,
    sum_recv,
    local_sem,
    q_sem,
    kvu_sem,
    kvd_sem,
    gu_sem,
    gd_sem,
    o_sem,
    lse_sem,
    head_sem,
    res_sem,
    upy_sem,
    upu_sem,
    upd_sem,
    dnu_sem,
    dnd_sem,
    dny_sem,
    pair_sem,
    sum_sem,
):
    nz, ny, nx, nc = sizes
    z, y, x, c = (lax.axis_index(name) for name in ("z", "y", "x", "c"))
    tp = x * nc + c
    tok, hd = q_all.shape[1], q_all.shape[2]
    own_rows, width = out_ref.shape
    to_exp2 = hd**-0.5 * math.log2(math.e)
    kv_up, kv_down = nz // 2, nz - 1 - nz // 2
    w_up, w_down = nz - 1 - nz // 2, nz // 2
    tiles = ny * tok // ROW_TILE
    per_block = tok // ROW_TILE

    def wrap(value, size):
        return lax.rem(value + size, size)

    above, below = {"z": wrap(z + 1, nz)}, {"z": wrap(z - 1, nz)}

    def y_peer(d):
        return {"y": wrap(y + d, ny)}

    tp_peers = [(dx, dc) for dx in range(nx) for dc in range(nc) if dx or dc]

    def tp_peer(dx, dc):
        return {"x": wrap(x + dx, nx), "c": wrap(c + dc, nc)}

    def tp_from(dx, dc):
        return wrap(x - dx, nx) * nc + wrap(c - dc, nc)

    locals_ = [
        pltpu.make_async_copy(src, dst, local_sem.at[i])
        for i, (src, dst) in enumerate(
            [
                (k_hbm, kv_all.at[z, 0]),
                (v_hbm, kv_all.at[z, 1]),
                (gate_hbm, gate_all.at[z]),
                (q_hbm, q_all.at[y]),
                (up_hbm, up_all.at[z, y]),
                (dn_hbm, dn_all.at[z, y]),
                (res_hbm, res_all.at[tp]),
                (wo_hbm, wo_s),
            ]
        )
    ]
    for copy in locals_:
        copy.start()

    barrier = pltpu.get_barrier_semaphore()
    peers = [above, below] + [y_peer(d) for d in range(1, ny)]
    peers += [tp_peer(dx, dc) for dx, dc in tp_peers]
    for peer in peers:
        pl.semaphore_signal(barrier, inc=1, device_id=peer, device_id_type=MESH)
    pl.semaphore_wait(barrier, len(peers))

    def kv_copy(slot, sems, gate_sems, step, device):
        return (
            remote(kv_all.at[slot], kv_all.at[slot], sems.at[0, step - 1], sems.at[1, step - 1], device),
            remote(
                gate_all.at[slot],
                gate_all.at[slot],
                gate_sems.at[0, step - 1],
                gate_sems.at[1, step - 1],
                device,
            ),
        )

    def kv_up_send(step):
        slot = z - step + 1
        return (slot >= 0) & (z < nz - 1), kv_copy(wrap(slot, nz), kvu_sem, gu_sem, step, above)

    def kv_up_recv(step):
        return z - step >= 0, kv_copy(wrap(z - step, nz), kvu_sem, gu_sem, step, above)

    def kv_down_send(step):
        slot = wrap(z + step - 1, nz)
        return slot < kv_down, kv_copy(slot, kvd_sem, gd_sem, step, below)

    def kv_down_recv(step):
        slot = wrap(z + step, nz)
        return slot < kv_down, kv_copy(slot, kvd_sem, gd_sem, step, below)

    def start(pair):
        when, copies = pair

        @pl.when(when)
        def _():
            for copy in copies:
                copy.start()

    def wait_recv(pair):
        when, copies = pair

        @pl.when(when)
        def _():
            for copy in copies:
                copy.wait_recv()

    def wait_send(pair):
        when, copies = pair

        @pl.when(when)
        def _():
            for copy in copies:
                copy.wait_send()

    def ring(buf, sems, step, device, slot):
        return remote(buf.at[slot], buf.at[slot], sems.at[0, step - 1], sems.at[1, step - 1], device)

    def upu(step, arriving=False):
        return ring(up_all, upu_sem, step, above, wrap(z - step + (0 if arriving else 1), nz))

    def upd(step, arriving=False):
        return ring(up_all, upd_sem, step, below, wrap(z + step - (0 if arriving else 1), nz))

    def dn_ring(sems, step, device, slot):
        ref = dn_all.at[slot, y]
        return remote(ref, ref, sems.at[0, step - 1], sems.at[1, step - 1], device)

    def dnu(step, arriving=False):
        return dn_ring(dnu_sem, step, above, wrap(z - step + (0 if arriving else 1), nz))

    def dnd(step, arriving=False):
        return dn_ring(dnd_sem, step, below, wrap(z + step - (0 if arriving else 1), nz))

    def y_copies(buf_at, sems, arriving=False):
        out = []
        for d in range(1, ny):
            ref = buf_at(wrap(y - d, ny) if arriving else y)
            out.append(remote(ref, ref, sems.at[0, d - 1], sems.at[1, d - 1], y_peer(d)))
        return out

    def dny(k, arriving=False):
        slot = wrap(z + k, nz)
        row = k + w_up
        return y_copies(lambda at: dn_all.at[slot, at], dny_sem.at[row], arriving)

    q_send = y_copies(lambda at: q_all.at[at], q_sem)
    q_arrive = y_copies(lambda at: q_all.at[at], q_sem, True)
    upy_send = y_copies(lambda at: up_all.at[z, at], upy_sem)
    upy_arrive = y_copies(lambda at: up_all.at[z, at], upy_sem, True)

    def tp_copies(buf, sems, arriving=False):
        out = []
        for i, (dx, dc) in enumerate(tp_peers):
            ref = buf.at[tp_from(dx, dc) if arriving else tp]
            out.append(remote(ref, ref, sems.at[0, i], sems.at[1, i], tp_peer(dx, dc)))
        return out

    res_send, res_arrive = tp_copies(res_all, res_sem), tp_copies(res_all, res_sem, True)
    head_send, head_arrive = tp_copies(heads, head_sem), tp_copies(heads, head_sem, True)

    def o_copies(arriving=False):
        out = []
        for d in range(1, ny):
            to = wrap(y + d, ny)
            source = wrap(y - d, ny) if arriving else y
            out.append(
                remote(o_send.at[to], o_recv.at[source], o_sem.at[0, d - 1], o_sem.at[1, d - 1], y_peer(d))
            )
            out.append(
                remote(
                    lse_send.at[to], lse_recv.at[source], lse_sem.at[0, d - 1], lse_sem.at[1, d - 1], y_peer(d)
                )
            )
        return out

    def start_all(copies):
        for copy in copies:
            copy.start()

    for copy in locals_[:3]:
        copy.wait()
    start(kv_up_send(1))
    start(kv_down_send(1))
    locals_[3].wait()
    start_all(q_send)
    locals_[4].wait()
    start_all(upy_send)
    locals_[5].wait()
    dnd(1).start()
    start_all(dny(0))
    locals_[6].wait()
    start_all(res_send)

    top_s[...] = jnp.full_like(top_s, LOW)
    acc_s[...] = jnp.zeros_like(acc_s)
    v_ones[:, hd:] = jnp.ones((tok, hd), jnp.bfloat16)

    def attend(slot, first_tile, masked):
        v_ones[:, :hd] = kv_all[slot, 1]

        def tile(t, carry):
            rows = pl.ds(t * ROW_TILE, ROW_TILE)
            q = q_all[t // per_block, pl.ds(lax.rem(t, per_block) * ROW_TILE, ROW_TILE), :]
            s = dot(q, kv_all[slot, 0], ((1,), (1,))) - gate_all[slot, 0:1, :] * (hd**0.5)
            if masked:
                q_pos = t * ROW_TILE + lax.broadcasted_iota(jnp.int32, s.shape, 0)
                k_pos = y * tok + lax.broadcasted_iota(jnp.int32, s.shape, 1)
                s = jnp.where(k_pos <= q_pos, s, LOW)
            old = top_s[rows, :]
            new = jnp.maximum(old, jnp.max(s, axis=1, keepdims=True))
            fade = jnp.exp2((old - new) * to_exp2)
            weights = jnp.exp2((s - jnp.concatenate([new] * (tok // hd), axis=1)) * to_exp2)
            product = dot(weights.astype(jnp.bfloat16), v_ones[...])
            acc_s[rows, :] = acc_s[rows, :] * jnp.concatenate([fade, fade], axis=1) + product
            top_s[rows, :] = new
            return carry

        lax.fori_loop(first_tile, tiles, tile, 0)

    for copy in q_arrive:
        copy.wait_recv()
    attend(z, y * per_block, True)

    for step in range(1, kv_up + 1):
        wait_recv(kv_up_recv(step))
        if step < kv_up:
            start(kv_up_send(step + 1))
        if step <= kv_down:
            wait_recv(kv_down_recv(step))
            if step < kv_down:
                start(kv_down_send(step + 1))
        if step == 1:
            for copy in upy_arrive:
                copy.wait_recv()
            upd(1).start()
        if step == kv_up - 1:
            dnu(1).start()
            upu(1).start()

        @pl.when(z - step >= 0)
        def _():
            attend(wrap(z - step, nz), 0, False)

        if step <= kv_down:

            @pl.when(z + step >= nz)
            def _():
                attend(wrap(z + step, nz), 0, False)

        if step <= w_down:
            dnd(step, True).wait_recv()
            if step < w_down:
                dnd(step + 1).start()
            if step <= 2:
                start_all(dny(step))
    upd(1, True).wait_recv()
    upd(2).start()

    eye = lax.broadcasted_iota(jnp.int32, (hd, hd), 0) == lax.broadcasted_iota(jnp.int32, (hd, hd), 1)

    for block in range(ny):
        for sub in range(tok // hd):
            rows = pl.ds(block * tok + sub * hd, hd)
            denom = jnp.maximum(acc_s[rows, hd:], 1e-30)
            o_send[block, sub * hd : (sub + 1) * hd, :] = (acc_s[rows, :hd] / denom).astype(jnp.bfloat16)
            lse = top_s[rows, :] * to_exp2 + jnp.log2(denom)
            line = jnp.sum(jnp.where(eye, lse, 0.0), axis=0, keepdims=True)
            lse_send[block, :, sub * hd : (sub + 1) * hd] = jnp.broadcast_to(line, (8, hd))
    start_all(o_copies())
    o_recv[y] = o_send[y]
    lse_recv[y] = lse_send[y]

    for step in range(3, w_down + 1):
        start_all(dny(step))
    dnu(1, True).wait_recv()
    dnu(2).start()
    start_all(dny(-1))

    for copy in o_copies(True):
        copy.wait_recv()
    for sub in range(tok // hd):
        span = slice(sub * hd, (sub + 1) * hd)
        lines = [lse_recv[i, 0:1, span] for i in range(ny)]
        best = functools.reduce(jnp.maximum, lines)
        shares = [jnp.exp2(line - best) for line in lines]
        total = functools.reduce(jnp.add, shares)
        summed = jnp.zeros((hd, hd), jnp.float32)
        for i in range(ny):
            share = jnp.broadcast_to(shares[i] / total, (hd, hd))
            column = jnp.sum(jnp.where(eye, share, 0.0), axis=1, keepdims=True)
            summed = summed + column * o_recv[i, span, :].astype(jnp.float32)
        heads[tp, span, :] = summed.astype(jnp.bfloat16)
    start_all(head_send)

    dnu(2, True).wait_recv()
    dnu(3).start()
    start_all(dny(-2))
    upu(1, True).wait_recv()
    upu(2).start()
    upd(2, True).wait_recv()
    upd(3).start()

    locals_[7].wait()
    for copy in res_arrive:
        copy.wait_recv()
    for copy in head_arrive:
        copy.wait_recv()
    n_heads = heads.shape[0]

    def project(n, squares):
        cols = pl.ds(pl.multiple_of(n * COL_TILE, COL_TILE), COL_TILE)
        attended = jnp.concatenate([heads[h] for h in range(n_heads)], axis=1)
        base = res_all[:, :, cols].reshape(tok, COL_TILE).astype(jnp.float32)
        total = base + dot(attended, wo_s[:, cols])
        rsum[:, cols] = total
        return squares + jnp.sum(total * total, axis=1, keepdims=True)

    squares = lax.fori_loop(0, width // COL_TILE, project, jnp.zeros((tok, 1), jnp.float32))
    inverse = lax.rsqrt(squares / width + 1e-06)
    top_s[0:tok, :] = jnp.broadcast_to(inverse, (tok, hd))

    def normalise(r, carry):
        rows = pl.ds(pl.multiple_of(r * own_rows, own_rows), own_rows)
        factor = top_s[rows, 0:1]
        normed[rows, :] = (rsum[rows, :] * factor * gain_ref[...]).astype(jnp.bfloat16)
        return carry

    lax.fori_loop(0, tok // own_rows, normalise, 0)

    upu(2, True).wait_recv()
    upu(3).start()
    upd(3, True).wait_recv()
    upd(4).start()
    dnu(3, True).wait_recv()
    start_all(dny(-3))

    upu(3, True).wait_recv()
    upd(4, True).wait_recv()
    ff = hidden.shape[1]

    def up_tile(n, carry):
        cols = pl.ds(pl.multiple_of(n * COL_TILE, COL_TILE), COL_TILE)
        proj = dot(normed[...], up_all[:, :, :, cols].reshape(width, COL_TILE))
        hidden[:, cols] = jnp.square(jnp.maximum(proj, 0.0)).astype(jnp.bfloat16)
        return carry

    lax.fori_loop(0, ff // COL_TILE, up_tile, 0)

    for k in range(-w_up, w_down + 1):
        for copy in dny(k, True):
            copy.wait_recv()

    group_cols = width // GROUPS
    z_per_group = nz // GROUPS
    z_cols = width // nz

    def pair_copy(g):
        cols = slice(g * group_cols, (g + 1) * group_cols)
        return remote(
            part.at[1 - c, :, :, cols],
            pair_recv.at[:, :, cols],
            pair_sem.at[0, g],
            pair_sem.at[1, g],
            {"c": 1 - c},
        )

    def sum_copy(g, d):
        cols = slice(g * group_cols, (g + 1) * group_cols)
        return remote(
            sum_send.at[d, :, cols],
            sum_recv.at[d, :, cols],
            sum_sem.at[0, g, d - 1],
            sum_sem.at[1, g, d - 1],
            {"x": wrap(x + d, nx)},
        )

    def finish_pair(g):
        cols = slice(g * group_cols, (g + 1) * group_cols)
        pair_copy(g).wait_recv()
        for d in range(1, nx):
            at = wrap(x + d, nx)
            both = part[c, at, :, cols].astype(jnp.float32) + pair_recv[at, :, cols].astype(jnp.float32)
            sum_send[d, :, cols] = both.astype(jnp.bfloat16)
            sum_copy(g, d).start()

    for g in range(GROUPS):

        def down_tile(i, carry, g=g):
            at = g * z_per_group + i
            cols = pl.ds(pl.multiple_of(at * z_cols, z_cols), z_cols)
            block = dot(hidden[...], dn_all[at].reshape(z_cols, ff), ((1,), (1,)))
            for owner in range(nx * nc):
                part[owner % nc, owner // nc, :, cols] = block[
                    owner * own_rows : (owner + 1) * own_rows, :
                ].astype(jnp.bfloat16)
            return carry

        lax.fori_loop(0, z_per_group, down_tile, 0)
        pair_copy(g).start()
        if g:
            finish_pair(g - 1)
    finish_pair(GROUPS - 1)

    final = rsum[pl.ds(pl.multiple_of(tp * own_rows, own_rows), own_rows), :]
    final = final + (part[c, x].astype(jnp.float32) + pair_recv[x].astype(jnp.float32))
    for g in range(GROUPS):
        for d in range(1, nx):
            sum_copy(g, d).wait_recv()
    for d in range(1, nx):
        final = final + sum_recv[d].astype(jnp.float32)
    out_ref[...] = final.astype(jnp.bfloat16)

    for step in range(1, kv_up + 1):
        wait_send(kv_up_send(step))
    for step in range(1, kv_down + 1):
        wait_send(kv_down_send(step))
    sent = q_send + upy_send + res_send + head_send + o_copies()
    for step in range(1, w_up + 1):
        sent += [upu(step), dnu(step)]
    for step in range(1, w_down + 1):
        sent += [upd(step), dnd(step)]
    for k in range(-w_up, w_down + 1):
        sent += dny(k)
    for g in range(GROUPS):
        sent += [pair_copy(g)] + [sum_copy(g, d) for d in range(1, nx)]
    for copy in sent:
        copy.wait_send()


def per_device(sizes, queries, keys, values, cum_gate, residual, w_out, gain, w_up, w_down):
    nz, ny, nx, nc = sizes
    ntp = nx * nc
    tok, hd = queries.shape
    rows, width = residual.shape
    depth, ff = w_up.shape
    gates = jnp.broadcast_to(cum_gate.reshape(1, tok), (8, tok))
    bf16, f32 = jnp.bfloat16, jnp.float32
    anywhere = pl.BlockSpec(memory_space=pl.ANY)
    in_vmem = pl.BlockSpec(memory_space=pltpu.VMEM)
    dma = pltpu.SemaphoreType.DMA
    up_steps, down_steps = nz // 2, nz - 1 - nz // 2
    return pl.pallas_call(
        functools.partial(layer_kernel, sizes),
        out_shape=jax.ShapeDtypeStruct((rows, width), bf16),
        in_specs=[anywhere] * 6 + [in_vmem] + [anywhere] * 2,
        out_specs=in_vmem,
        scratch_shapes=[
            pltpu.VMEM((ny, tok, hd), bf16),
            pltpu.VMEM((nz, 2, tok, hd), bf16),
            pltpu.VMEM((nz, 8, tok), f32),
            pltpu.VMEM((tok, 2 * hd), bf16),
            pltpu.VMEM((ny * tok, hd), f32),
            pltpu.VMEM((ny * tok, 2 * hd), f32),
            pltpu.VMEM((ny, tok, hd), bf16),
            pltpu.VMEM((ny, tok, hd), bf16),
            pltpu.VMEM((ny, 8, tok), f32),
            pltpu.VMEM((ny, 8, tok), f32),
            pltpu.VMEM((ntp, tok, hd), bf16),
            pltpu.VMEM((ntp, rows, width), bf16),
            pltpu.VMEM(w_out.shape, bf16),
            pltpu.VMEM((tok, width), f32),
            pltpu.VMEM((tok, width), bf16),
            pltpu.VMEM((nz, ny, depth, ff), bf16),
            pltpu.VMEM((nz, ny, depth, ff), bf16),
            pltpu.VMEM((tok, ff), bf16),
            pltpu.VMEM((nc, nx, rows, width), bf16),
            pltpu.VMEM((nx, rows, width), bf16),
            pltpu.VMEM((nx, rows, width), bf16),
            pltpu.VMEM((nx, rows, width), bf16),
            dma((8,)),
            dma((2, ny - 1)),
            dma((2, up_steps)),
            dma((2, down_steps)),
            dma((2, up_steps)),
            dma((2, down_steps)),
            dma((2, ny - 1)),
            dma((2, ny - 1)),
            dma((2, ntp - 1)),
            dma((2, ntp - 1)),
            dma((2, ny - 1)),
            dma((2, down_steps)),
            dma((2, up_steps)),
            dma((2, down_steps)),
            dma((2, up_steps)),
            dma((nz, 2, ny - 1)),
            dma((2, GROUPS)),
            dma((2, GROUPS, nx - 1)),
        ],
        compiler_params=pltpu.CompilerParams(
            collective_id=0, has_side_effects=True, vmem_limit_bytes=63 * 1024 * 1024
        ),
    )(queries, keys, values, gates, residual, w_out, gain.reshape(1, width), w_up, w_down.T)


def solution(mesh):
    finer = Mesh(mesh.devices.reshape(GRID), ("z", "y", "x", "c"))
    sp, tp = ("z", "y"), ("x", "c")
    rows = ("z", "y", "x", "c")
    in_specs = (
        P(sp, tp),
        P(sp, tp),
        P(sp, tp),
        P(sp, tp),
        P(rows, None),
        P(),
        P(),
        P(sp, tp),
        P(tp, sp),
    )
    return jax.shard_map(
        functools.partial(per_device, GRID),
        mesh=finer,
        in_specs=in_specs,
        out_specs=P(rows, None),
        check_vma=False,
    )
```

time: 315 us -> 125 us (0.40)
  Pallas kernels: 0 us -> 122 us
  waiting for transfers between devices: 92 us -> 0 us
  blocking collectives: 67.5 us -> 0 us
  matrix products: 60.3 us -> 0 us
  other arithmetic: 32.6 us -> 0 us
  loops' own time: 16 us -> 0 us
  local copies, waits for them, and re-layouts: 18 us -> 2.96 us
  starting transfers between devices: 13.9 us -> 0 us
  between operations: 13.3 us -> 0.01 us
    pallas_call x0 -> x1, Pallas kernels: none -> 122 us  [per_device(): pl.pallas_call(functools.partial(layer_kernel, sizes), out_shape=jax.Shap...]
    all_gather x3 -> x0, waiting for transfers between devices: 65.7 us -> none  [the longest x1 65.7 us: sent_together(): filled = lax.all_gather(both, axis, axis=dim, tiled=True)]
    dot_general x18 -> x0, matrix products: 60.3 us -> none  [the longest x8 32.3 us: absorb_block(): jnp.einsum('qhd,khd->qhk', query_heads, key_blk, preferred_element_type=j...]
    all_to_all x2 -> x0, blocking collectives: 41.3 us -> none  [the longest x1 30.6 us: sum_at_owner(): lax.all_to_all(tiles, axis, split_axis=0, concat_axis=0, tiled=True)]
    all_to_all x2 -> x0, waiting for transfers between devices: 26.2 us -> none  [copy_for_each(): lax.all_to_all(jnp.broadcast_to(shard[None], (devices, *shard.shape)), ax...]
    all_gather x2 -> x0, blocking collectives: 26.2 us -> none  [whole_of(): filled = lax.all_gather(filled, axes[number], axis=dim, tiled=True)]
    reduce_sum x9 -> x0, other arithmetic: 24.4 us -> none  [the longest x8 24.1 us: absorb_block(): running_sum = running_sum * rescale + jnp.sum(weights, axis=-1)]
    another operation x1 -> x0, loops' own time: 16 us -> none  [per_device(): lax.scan(absorb_block, carried, (key_blocks, value_blocks, first_pos))]
  transfers between devices with their start and end apart: 5 -> 0, of which waited for: 2 -> 0; matrix products, arithmetic and copies ran while one was open for 30% -> 0% of each run, Pallas kernels for 0% -> 0%
where the time goes in v1:
time: 125 us; the launch traced here: 124 us
  Pallas kernels  122 us (98%)
  local copies, waits for them, and re-layouts  2.96 us (2%)
    pallas_call x1, Pallas kernels, per_device(): pl.pallas_call(functools.partial(layer_kernel, sizes), out_shape=jax.Shap...  122 us

profile of v1, /device:TPU:1, one launch (start us, length us, event | category | flops | bytes accessed | tf_op | source)
XLA Modules:
  0.0 124.5 jit_solution(1118483497450365401)
XLA Ops:
  0.0 1.3 %broadcast_in_dim.8.gate_hbm = f32[8,512]{1,0:T(8,128)} broadcast(f32[512]{0:T(512)} %bitcast.5), dimensions={1} | broadcast | bytes 18432 | tf_op jit(solution)/shard_map/broadcast_in_dim | solution.py:512
  1.3 121.5 %shard_map.91 = bf16[64,2048]{1,0:T(8,128)(2,1)} custom-call(bf16[512,128]{1,0:T(8,128)(2,1)} %q_hbm.1, bf16[512,128]{1,0:T(8,128)(2,1)} %k_hbm.1, bf16[512,128]{1,0:T(8,128)(2,1)} %v_hbm.1, f32[8,512]{1,0:T(8,128)} %broadcast_in_dim.8.gate_hbm, bf16[64,2048]{1,0:T(8,128)(2,1)} %res_hbm.1, bf16[1024,2048]{1,0:T(8,128)(2,1)} %wo_hbm.1, f32[1,2048]{1,0:T(1,128)} %bitcast.4, ...), custom_call_target="tpu_custom_call" | custom-call | tf_op jit(solution)/shard_map/pallas_call | solution.py:518
  122.8 1.7 %copy.11 = bf16[64,2048]{1,0:T(8,128)(2,1)} copy(bf16[64,2048]{1,0:T(8,128)(2,1)} %shard_map.91) | data formatting | bytes 524288

commit v2 on v1

v2 whole, which is shorter than its diff:
```python
import functools
import math

import jax
import jax.numpy as jnp
from jax import lax
from jax.experimental import pallas as pl
from jax.experimental.pallas import tpu as pltpu
from jax.sharding import Mesh
from jax.sharding import PartitionSpec as P

MESH = pl.DeviceIdType.MESH
GRID = (8, 4, 4, 2)
ROW_TILE = 256
COL_TILE = 256
FIRST_ROWS = 32
LOW = -1e30


def remote(src, dst, send_sem, recv_sem, device):
    return pltpu.make_async_remote_copy(
        src_ref=src,
        dst_ref=dst,
        send_sem=send_sem,
        recv_sem=recv_sem,
        device_id=device,
        device_id_type=MESH,
    )


def dot(a, b, contract=((1,), (0,))):
    return lax.dot_general(a, b, (contract, ((), ())), preferred_element_type=jnp.float32)


def layer_kernel(
    sizes,
    q_hbm,
    k_hbm,
    v_hbm,
    gate_hbm,
    res_hbm,
    wo_hbm,
    gain_ref,
    up_hbm,
    dn_hbm,
    out_ref,
    q_all,
    kv_all,
    gate_all,
    v_ones,
    top_s,
    acc_s,
    o_send,
    o_recv,
    lse_send,
    lse_recv,
    heads,
    res_all,
    wo_s,
    rsum,
    normed,
    up_all,
    dn_all,
    hidden,
    part,
    pair_recv,
    sum_send,
    sum_recv,
    local_sem,
    q_sem,
    kvu_sem,
    kvd_sem,
    gu_sem,
    gd_sem,
    vu_sem,
    vd_sem,
    o_sem,
    lse_sem,
    head_sem,
    pair_head_sem,
    res_sem,
    upy_sem,
    upu_sem,
    upd_sem,
    dnu_sem,
    dnd_sem,
    dny_sem,
    dnh_sem,
    u2u_sem,
    u2d_sem,
    u2y_sem,
    u2h_sem,
    pair_sem,
    sum_sem,
):
    nz, ny, nx, nc = sizes
    z, y, x, c = (lax.axis_index(name) for name in ("z", "y", "x", "c"))
    tp = x * nc + c
    tok, hd = q_all.shape[1], q_all.shape[2]
    own_rows, width = out_ref.shape
    to_exp2 = hd**-0.5 * math.log2(math.e)
    kv_up, kv_down = nz // 2, nz - 1 - nz // 2
    w_up, w_down = nz - 1 - nz // 2, nz // 2
    tiles = ny * tok // ROW_TILE
    per_block = tok // ROW_TILE

    def wrap(value, size):
        return lax.rem(value + size, size)

    above, below = {"z": wrap(z + 1, nz)}, {"z": wrap(z - 1, nz)}

    def y_peer(d):
        return {"y": wrap(y + d, ny)}

    tp_peers = [(dx, dc) for dx in range(nx) for dc in range(nc) if dx or dc]

    def tp_peer(dx, dc):
        return {"x": wrap(x + dx, nx), "c": wrap(c + dc, nc)}

    def tp_from(dx, dc):
        return wrap(x - dx, nx) * nc + wrap(c - dc, nc)

    locals_ = [
        pltpu.make_async_copy(src, dst, local_sem.at[i])
        for i, (src, dst) in enumerate(
            [
                (k_hbm, kv_all.at[z, 0]),
                (v_hbm, kv_all.at[z, 1]),
                (gate_hbm, gate_all.at[z]),
                (q_hbm, q_all.at[y]),
                (up_hbm, up_all.at[z, y]),
                (dn_hbm, dn_all.at[z, y]),
                (res_hbm, res_all.at[tp]),
                (wo_hbm, wo_s),
            ]
        )
    ]
    for copy in locals_:
        copy.start()

    barrier = pltpu.get_barrier_semaphore()
    peers = [above, below] + [y_peer(d) for d in range(1, ny)]
    peers += [tp_peer(dx, dc) for dx, dc in tp_peers]
    for peer in peers:
        pl.semaphore_signal(barrier, inc=1, device_id=peer, device_id_type=MESH)
    pl.semaphore_wait(barrier, len(peers))

    def kv_copy(which, slot, up, step, device):
        ref = kv_all.at[slot, which]
        sems = ((kvu_sem, vu_sem) if up else (kvd_sem, vd_sem))[which]
        copies = (remote(ref, ref, sems.at[0, step - 1], sems.at[1, step - 1], device),)
        if which == 0:
            ref, sems = gate_all.at[slot], gu_sem if up else gd_sem
            copies += (remote(ref, ref, sems.at[0, step - 1], sems.at[1, step - 1], device),)
        return copies

    def kv_up_send(which, step):
        slot = z - step + 1
        return (slot >= 0) & (z < nz - 1), kv_copy(which, wrap(slot, nz), True, step, above)

    def kv_up_recv(which, step):
        return z - step >= 0, kv_copy(which, wrap(z - step, nz), True, step, above)

    def kv_down_send(which, step):
        slot = wrap(z + step - 1, nz)
        return slot < kv_down, kv_copy(which, slot, False, step, below)

    def kv_down_recv(which, step):
        slot = wrap(z + step, nz)
        return slot < kv_down, kv_copy(which, slot, False, step, below)

    def start(pair):
        when, copies = pair

        @pl.when(when)
        def _():
            for copy in copies:
                copy.start()

    def wait_recv(pair):
        when, copies = pair

        @pl.when(when)
        def _():
            for copy in copies:
                copy.wait_recv()

    def wait_send(pair):
        when, copies = pair

        @pl.when(when)
        def _():
            for copy in copies:
                copy.wait_send()

    def up_ring(sems, d, step, device, slot):
        ref = up_all.at[slot, wrap(y - d, ny), 0:FIRST_ROWS, :]
        return remote(ref, ref, sems.at[0, step - 1, d], sems.at[1, step - 1, d], device)

    def upu(d, step, arriving=False):
        return up_ring(upu_sem, d, step, above, wrap(z - step + (0 if arriving else 1), nz))

    def upd(d, step, arriving=False):
        return up_ring(upd_sem, d, step, below, wrap(z + step - (0 if arriving else 1), nz))

    def pass_upu(d, step):
        upu(d, step, True).wait_recv()
        if step < w_up:
            upu(d, step + 1).start()

    def pass_upd(d, step):
        upd(d, step, True).wait_recv()
        if step < w_down:
            upd(d, step + 1).start()

    def pass_dnu(step):
        for copy in dnu(step, True):
            copy.wait_recv()
        if step < w_up:
            start_all(dnu(step + 1))

    def pass_dnd(step):
        for copy in dnd(step, True):
            copy.wait_recv()
        if step < w_down:
            start_all(dnd(step + 1))

    def rest_ring(sems, rest_sems, step, device, slot):
        out = []
        for ref, s in ((dn_all.at[slot, y], sems), (up_all.at[slot, y, FIRST_ROWS:, :], rest_sems)):
            out.append(remote(ref, ref, s.at[0, step - 1], s.at[1, step - 1], device))
        return out

    def dnu(step, arriving=False):
        slot = wrap(z - step + (0 if arriving else 1), nz)
        return rest_ring(dnu_sem, u2u_sem, step, above, slot)

    def dnd(step, arriving=False):
        slot = wrap(z + step - (0 if arriving else 1), nz)
        return rest_ring(dnd_sem, u2d_sem, step, below, slot)

    def y_copies(buf_at, sems, arriving=False):
        out = []
        for d in range(1, ny):
            ref = buf_at(wrap(y - d, ny) if arriving else y)
            out.append(remote(ref, ref, sems.at[0, d - 1], sems.at[1, d - 1], y_peer(d)))
        return out

    rest_rows = slice(FIRST_ROWS, up_all.shape[2])

    def over_y(rest, k, side, arriving=False, half=False):
        buf, rows = (up_all, rest_rows) if rest else (dn_all, slice(0, dn_all.shape[2]))
        i = (1 - side) // 2
        source = y - side * ((1 if half else 0) + (1 if arriving else 0))
        if half:
            mid = (rows.start + rows.stop) // 2
            rows = slice(mid, rows.stop) if i else slice(rows.start, mid)
        ref = buf.at[wrap(z + k, nz), wrap(source, ny), rows, :]
        sems = (u2h_sem if rest else dnh_sem) if half else (u2y_sem if rest else dny_sem)
        sems = sems.at[k + w_up]
        return remote(ref, ref, sems.at[0, i], sems.at[1, i], y_peer(side))

    def send_y(k):
        for rest in (True, False):
            for side in (1, -1):
                over_y(rest, k, side).start()

    def pass_y(k):
        for rest in (True, False):
            for side in (1, -1):
                over_y(rest, k, side, True).wait_recv()
                over_y(rest, k, side, half=True).start()

    q_send = y_copies(lambda at: q_all.at[at], q_sem)
    q_arrive = y_copies(lambda at: q_all.at[at], q_sem, True)
    upy_send = y_copies(lambda at: up_all.at[z, at, 0:FIRST_ROWS, :], upy_sem)
    upy_arrive = y_copies(lambda at: up_all.at[z, at, 0:FIRST_ROWS, :], upy_sem, True)

    def tp_copies(buf, sems, arriving=False):
        out = []
        for i, (dx, dc) in enumerate(tp_peers):
            ref = buf.at[tp_from(dx, dc) if arriving else tp]
            out.append(remote(ref, ref, sems.at[0, i], sems.at[1, i], tp_peer(dx, dc)))
        return out

    res_send, res_arrive = tp_copies(res_all, res_sem), tp_copies(res_all, res_sem, True)

    def head_copy(d, arriving=False):
        ref = heads.at[wrap(x - d, nx) * nc + c if arriving else tp]
        return remote(ref, ref, head_sem.at[0, d - 1], head_sem.at[1, d - 1], {"x": wrap(x + d, nx)})

    def head_to_pair(d, arriving=False):
        ref = heads.at[wrap(x - d, nx) * nc + (1 - c if arriving else c)]
        return remote(ref, ref, pair_head_sem.at[0, d], pair_head_sem.at[1, d], {"c": 1 - c})

    def o_copies(arriving=False):
        out = []
        for d in range(1, ny):
            to = wrap(y + d, ny)
            source = wrap(y - d, ny) if arriving else y
            out.append(
                remote(o_send.at[to], o_recv.at[source], o_sem.at[0, d - 1], o_sem.at[1, d - 1], y_peer(d))
            )
            out.append(
                remote(
                    lse_send.at[to], lse_recv.at[source], lse_sem.at[0, d - 1], lse_sem.at[1, d - 1], y_peer(d)
                )
            )
        return out

    def start_all(copies):
        for copy in copies:
            copy.start()

    locals_[0].wait()
    locals_[2].wait()
    start(kv_up_send(0, 1))
    start(kv_down_send(0, 1))
    locals_[1].wait()
    start(kv_up_send(1, 1))
    start(kv_down_send(1, 1))
    locals_[3].wait()
    start_all(q_send)
    locals_[4].wait()
    locals_[5].wait()
    start_all(dnd(1))
    start_all(dnu(1))
    upd(0, 1).start()
    start_all(upy_send)
    send_y(0)
    locals_[6].wait()
    start_all(res_send)

    top_s[...] = jnp.full_like(top_s, LOW)
    acc_s[...] = jnp.zeros_like(acc_s)
    v_ones[:, hd:] = jnp.ones((tok, hd), jnp.bfloat16)

    def attend(slot, first_tile, count, masked=False):
        for t in [first_tile + u for u in range(count)]:
            rows = pl.ds(t * ROW_TILE, ROW_TILE)
            q = q_all[t // per_block, pl.ds(lax.rem(t, per_block) * ROW_TILE, ROW_TILE), :]
            s = dot(q, kv_all[slot, 0], ((1,), (1,))) - gate_all[slot] * (hd**0.5)
            if masked:
                q_pos = t * ROW_TILE + lax.broadcasted_iota(jnp.int32, s.shape, 0)
                k_pos = y * tok + lax.broadcasted_iota(jnp.int32, s.shape, 1)
                s = jnp.where(k_pos <= q_pos, s, LOW)
            old = top_s[rows, :]
            new = jnp.maximum(old, jnp.max(s, axis=1, keepdims=True))
            fade = jnp.exp2((old - new) * to_exp2)
            weights = jnp.exp2((s - jnp.concatenate([new] * (tok // hd), axis=1)) * to_exp2)
            product = dot(weights.astype(jnp.bfloat16), v_ones[...])
            acc_s[rows, :] = acc_s[rows, :] * jnp.concatenate([fade, fade], axis=1) + product
            top_s[rows, :] = new

    v_ones[:, :hd] = kv_all[z, 1]
    attend(z, y * per_block, per_block, True)
    for copy in q_arrive:
        copy.wait_recv()

    def later_block(b, carry):
        attend(z, b * per_block, per_block)
        return carry

    lax.fori_loop(y + 1, ny, later_block, 0)

    def forward_kv(step):
        for which in range(2):
            wait_recv(kv_up_recv(which, step))
            if step < kv_up:
                start(kv_up_send(which, step + 1))
            if step <= kv_down:
                wait_recv(kv_down_recv(which, step))
                if step < kv_down:
                    start(kv_down_send(which, step + 1))

    def attend_step(step):
        first = jnp.where(z - step >= 0, 0, 1)
        last = jnp.where(z + step >= nz, 2, 1) if step <= kv_down else 1

        def block(u, carry):
            slot = wrap(z + (2 * u - 1) * step, nz)
            v_ones[:, :hd] = kv_all[slot, 1]
            attend(slot, 0, tiles)
            return carry

        lax.fori_loop(first, last, block, 0)

    forward_kv(1)
    for d in range(1, ny):
        upy_arrive[d - 1].wait_recv()
        upd(d, 1).start()
    attend_step(1)
    pass_dnd(1)
    pass_dnu(1)
    send_y(1)
    send_y(-1)
    pass_y(0)

    forward_kv(2)
    pass_upd(0, 1)
    attend_step(2)
    pass_dnd(2)
    pass_dnu(2)
    send_y(2)
    send_y(-2)
    pass_y(1)

    forward_kv(3)
    for d in range(ny):
        upu(d, 1).start()
    pass_upd(1, 1)
    attend_step(3)
    pass_upd(2, 1)
    pass_dnd(3)
    pass_dnu(3)
    pass_y(-1)

    forward_kv(4)
    pass_upd(3, 1)
    pass_upd(0, 2)
    attend_step(4)
    pass_upd(1, 2)
    pass_upd(2, 2)
    pass_y(2)

    eye = lax.broadcasted_iota(jnp.int32, (hd, hd), 0) == lax.broadcasted_iota(jnp.int32, (hd, hd), 1)

    for block in range(ny):
        for sub in range(tok // hd):
            rows = pl.ds(block * tok + sub * hd, hd)
            denom = jnp.maximum(acc_s[rows, hd:], 1e-30)
            o_send[block, sub * hd : (sub + 1) * hd, :] = (acc_s[rows, :hd] / denom).astype(jnp.bfloat16)
            lse = top_s[rows, :] * to_exp2 + jnp.log2(denom)
            line = jnp.sum(jnp.where(eye, lse, 0.0), axis=0, keepdims=True)
            lse_send[block, :, sub * hd : (sub + 1) * hd] = line
    start_all(o_copies())
    o_recv[y] = o_send[y]
    lse_recv[y] = lse_send[y]

    pass_dnd(4)
    for k in (3, -3, 4):
        send_y(k)
    pass_y(-2)
    pass_upu(0, 1)
    pass_upu(1, 1)
    pass_upd(3, 2)

    for copy in o_copies(True):
        copy.wait_recv()
    for sub in range(tok // hd):
        span = slice(sub * hd, (sub + 1) * hd)
        lines = [lse_recv[i, 0:1, span] for i in range(ny)]
        best = functools.reduce(jnp.maximum, lines)
        shares = [jnp.exp2(line - best) for line in lines]
        total = functools.reduce(jnp.add, shares)
        summed = jnp.zeros((hd, hd), jnp.float32)
        for i in range(ny):
            share = jnp.broadcast_to(shares[i] / total, (hd, hd))
            column = jnp.sum(jnp.where(eye, share, 0.0), axis=1, keepdims=True)
            summed = summed + column * o_recv[i, span, :].astype(jnp.float32)
        heads[tp, span, :] = summed.astype(jnp.bfloat16)
    for d in range(1, nx):
        head_copy(d).start()
    head_to_pair(0).start()

    pass_upu(2, 1)
    pass_upu(3, 1)
    pass_upd(0, 3)
    pass_upd(1, 3)
    pass_y(3)

    locals_[7].wait()
    for copy in res_arrive:
        copy.wait_recv()
    for d in range(1, nx):
        head_copy(d, True).wait_recv()
        head_to_pair(d).start()
    pass_upu(0, 2)
    pass_upd(2, 3)
    pass_y(-3)
    for d in range(nx):
        head_to_pair(d, True).wait_recv()
    n_heads = heads.shape[0]

    def project(n, squares):
        cols = pl.ds(pl.multiple_of(n * COL_TILE, COL_TILE), COL_TILE)
        attended = jnp.concatenate([heads[h] for h in range(n_heads)], axis=1)
        base = res_all[:, :, cols].reshape(tok, COL_TILE).astype(jnp.float32)
        total = base + dot(attended, wo_s[:, cols])
        rsum[:, cols] = total
        return squares + jnp.sum(total * total, axis=1, keepdims=True)

    squares = jnp.zeros((tok, 1), jnp.float32)
    segment = width // COL_TILE // 4
    for i in range(4):
        squares = lax.fori_loop(i * segment, (i + 1) * segment, project, squares)
        if i < 3:
            pass_upu(i + 1, 2)
        else:
            pass_upd(3, 3)
    inverse = lax.rsqrt(squares / width + 1e-06)
    top_s[0:tok, :] = jnp.broadcast_to(inverse, (tok, hd))

    def normalise(r, carry):
        rows = pl.ds(pl.multiple_of(r * own_rows, own_rows), own_rows)
        factor = top_s[rows, 0:1]
        normed[rows, :] = (rsum[rows, :] * factor * gain_ref[...]).astype(jnp.bfloat16)
        return carry

    lax.fori_loop(0, tok // own_rows, normalise, 0)

    pass_y(4)

    for k in range(-w_up, w_down + 1):
        for side in (1, -1):
            over_y(True, k, side, True, True).wait_recv()
    for d in range(ny):
        pass_upu(d, 3)
        pass_upd(d, 4)
    ff = hidden.shape[1]

    def up_tile(n, carry):
        cols = pl.ds(pl.multiple_of(n * COL_TILE, COL_TILE), COL_TILE)
        proj = dot(normed[...], up_all[:, :, :, cols].reshape(width, COL_TILE))
        hidden[:, cols] = jnp.square(jnp.maximum(proj, 0.0)).astype(jnp.bfloat16)
        return carry

    lax.fori_loop(0, ff // COL_TILE, up_tile, 0)

    z_cols = width // nz
    order = [0] + [s for k in range(1, w_up + 1) for s in (k, -k)] + list(range(w_up + 1, w_down + 1))

    def cols_of(k):
        return pl.ds(pl.multiple_of(wrap(z + k, nz) * z_cols, z_cols), z_cols)

    def pair_copy(k):
        return remote(
            part.at[1 - c, :, :, cols_of(k)],
            pair_recv.at[:, :, cols_of(k)],
            pair_sem.at[0, k + w_up],
            pair_sem.at[1, k + w_up],
            {"c": 1 - c},
        )

    def sum_copy(k, d):
        return remote(
            sum_send.at[d, :, cols_of(k)],
            sum_recv.at[d, :, cols_of(k)],
            sum_sem.at[0, k + w_up, d - 1],
            sum_sem.at[1, k + w_up, d - 1],
            {"x": wrap(x + d, nx)},
        )

    def finish_pair(k):
        cols = cols_of(k)
        pair_copy(k).wait_recv()
        for d in range(1, nx):
            at = wrap(x + d, nx)
            both = part[c, at, :, cols].astype(jnp.float32) + pair_recv[at, :, cols].astype(jnp.float32)
            sum_send[d, :, cols] = both.astype(jnp.bfloat16)
            sum_copy(k, d).start()

    for i, k in enumerate(order):
        for side in (1, -1):
            over_y(False, k, side, True, True).wait_recv()
        block = dot(hidden[...], dn_all[wrap(z + k, nz)].reshape(z_cols, ff), ((1,), (1,)))
        for owner in range(nx * nc):
            part[owner % nc, owner // nc, :, cols_of(k)] = block[
                owner * own_rows : (owner + 1) * own_rows, :
            ].astype(jnp.bfloat16)
        pair_copy(k).start()
        if i:
            finish_pair(order[i - 1])
    finish_pair(order[-1])

    final = rsum[pl.ds(pl.multiple_of(tp * own_rows, own_rows), own_rows), :]
    final = final + (part[c, x].astype(jnp.float32) + pair_recv[x].astype(jnp.float32))
    for k in order:
        for d in range(1, nx):
            sum_copy(k, d).wait_recv()
    for d in range(1, nx):
        final = final + sum_recv[d].astype(jnp.float32)
    out_ref[...] = final.astype(jnp.bfloat16)

    for which in range(2):
        for step in range(1, kv_up + 1):
            wait_send(kv_up_send(which, step))
        for step in range(1, kv_down + 1):
            wait_send(kv_down_send(which, step))
    sent = q_send + upy_send + res_send + o_copies()
    sent += [head_copy(d) for d in range(1, nx)] + [head_to_pair(d) for d in range(nx)]
    for step in range(1, w_up + 1):
        sent += dnu(step) + [upu(d, step) for d in range(ny)]
    for step in range(1, w_down + 1):
        sent += dnd(step) + [upd(d, step) for d in range(ny)]
    for k in order:
        for rest in (True, False):
            for side in (1, -1):
                sent += [over_y(rest, k, side), over_y(rest, k, side, half=True)]
        sent += [pair_copy(k)] + [sum_copy(k, d) for d in range(1, nx)]
    for copy in sent:
        copy.wait_send()


def per_device(sizes, queries, keys, values, cum_gate, residual, w_out, gain, w_up, w_down):
    nz, ny, nx, nc = sizes
    ntp = nx * nc
    tok, hd = queries.shape
    rows, width = residual.shape
    depth, ff = w_up.shape
    gates = cum_gate.reshape(1, tok)
    bf16, f32 = jnp.bfloat16, jnp.float32
    anywhere = pl.BlockSpec(memory_space=pl.ANY)
    in_vmem = pl.BlockSpec(memory_space=pltpu.VMEM)
    dma = pltpu.SemaphoreType.DMA
    up_steps, down_steps = nz // 2, nz - 1 - nz // 2
    return pl.pallas_call(
        functools.partial(layer_kernel, sizes),
        out_shape=jax.ShapeDtypeStruct((rows, width), bf16),
        in_specs=[anywhere] * 6 + [in_vmem] + [anywhere] * 2,
        out_specs=in_vmem,
        scratch_shapes=[
            pltpu.VMEM((ny, tok, hd), bf16),
            pltpu.VMEM((nz, 2, tok, hd), bf16),
            pltpu.VMEM((nz, 1, tok), f32),
            pltpu.VMEM((tok, 2 * hd), bf16),
            pltpu.VMEM((ny * tok, hd), f32),
            pltpu.VMEM((ny * tok, 2 * hd), f32),
            pltpu.VMEM((ny, tok, hd), bf16),
            pltpu.VMEM((ny, tok, hd), bf16),
            pltpu.VMEM((ny, 1, tok), f32),
            pltpu.VMEM((ny, 1, tok), f32),
            pltpu.VMEM((ntp, tok, hd), bf16),
            pltpu.VMEM((ntp, rows, width), bf16),
            pltpu.VMEM(w_out.shape, bf16),
            pltpu.VMEM((tok, width), f32),
            pltpu.VMEM((tok, width), bf16),
            pltpu.VMEM((nz, ny, depth, ff), bf16),
            pltpu.VMEM((nz, ny, depth, ff), bf16),
            pltpu.VMEM((tok, ff), bf16),
            pltpu.VMEM((nc, nx, rows, width), bf16),
            pltpu.VMEM((nx, rows, width), bf16),
            pltpu.VMEM((nx, rows, width), bf16),
            pltpu.VMEM((nx, rows, width), bf16),
            dma((8,)),
            dma((2, ny - 1)),
            dma((2, up_steps)),
            dma((2, down_steps)),
            dma((2, up_steps)),
            dma((2, down_steps)),
            dma((2, up_steps)),
            dma((2, down_steps)),
            dma((2, ny - 1)),
            dma((2, ny - 1)),
            dma((2, nx - 1)),
            dma((2, nx)),
            dma((2, ntp - 1)),
            dma((2, ny - 1)),
            dma((2, down_steps, ny)),
            dma((2, up_steps, ny)),
            dma((2, down_steps)),
            dma((2, up_steps)),
            dma((nz, 2, 2)),
            dma((nz, 2, 2)),
            dma((2, down_steps)),
            dma((2, up_steps)),
            dma((nz, 2, 2)),
            dma((nz, 2, 2)),
            dma((2, nz)),
            dma((2, nz, nx - 1)),
        ],
        compiler_params=pltpu.CompilerParams(
            collective_id=0, has_side_effects=True, vmem_limit_bytes=63 * 1024 * 1024
        ),
    )(queries, keys, values, gates, residual, w_out, gain.reshape(1, width), w_up, w_down.T)


def solution(mesh):
    finer = Mesh(mesh.devices.reshape(GRID), ("z", "y", "x", "c"))
    sp, tp = ("z", "y"), ("x", "c")
    rows = ("z", "y", "x", "c")
    in_specs = (
        P(sp, tp),
        P(sp, tp),
        P(sp, tp),
        P(sp, tp),
        P(rows, None),
        P(),
        P(),
        P(sp, tp),
        P(tp, sp),
    )
    return jax.shard_map(
        functools.partial(per_device, GRID),
        mesh=finer,
        in_specs=in_specs,
        out_specs=P(rows, None),
        check_vma=False,
    )
```

time: 125 us -> 105 us (0.84)
  Pallas kernels: 122 us -> 103 us
  local copies, waits for them, and re-layouts: 2.96 us -> 1.67 us
    pallas_call x1, Pallas kernels: 122 us -> 103 us  [per_device(): pl.pallas_call(functools.partial(layer_kernel, sizes), out_shape=jax.Shap...]
    broadcast_in_dim x1 -> x0, local copies, waits for them, and re-layouts: 1.29 us -> none  [per_device(): gates = jnp.broadcast_to(cum_gate.reshape(1, tok), (8, tok))]
where the time goes in v2:
time: 105 us; the launch traced here: 104 us
  Pallas kernels  103 us (98%)
  local copies, waits for them, and re-layouts  1.67 us (2%)
    pallas_call x1, Pallas kernels, per_device(): pl.pallas_call(functools.partial(layer_kernel, sizes), out_shape=jax.Shap...  103 us

profile of v2, /device:TPU:1, one launch (start us, length us, event | category | flops | bytes accessed | tf_op | source)
XLA Modules:
  0.0 104.5 jit_solution(2536549336964858728)
XLA Ops:
  0.0 102.8 %shard_map.91 = bf16[64,2048]{1,0:T(8,128)(2,1)} custom-call(bf16[512,128]{1,0:T(8,128)(2,1)} %q_hbm.1, bf16[512,128]{1,0:T(8,128)(2,1)} %k_hbm.1, bf16[512,128]{1,0:T(8,128)(2,1)} %v_hbm.1, f32[1,512]{1,0:T(1,128)} %bitcast.5, bf16[64,2048]{1,0:T(8,128)(2,1)} %res_hbm.1, bf16[1024,2048]{1,0:T(8,128)(2,1)} %wo_hbm.1, f32[1,2048]{1,0:T(1,128)} %bitcast.4, ...), custom_call_target="tpu_custom_call" | custom-call | tf_op jit(solution)/shard_map/pallas_call | solution.py:617
  102.8 1.7 %copy.11 = bf16[64,2048]{1,0:T(8,128)(2,1)} copy(bf16[64,2048]{1,0:T(8,128)(2,1)} %shard_map.91) | data formatting | bytes 524288

commit v3 on v2

--- a/solution.py
+++ b/solution.py
@@ -15,6 +15,37 @@
 COL_TILE = 256
 FIRST_ROWS = 32
 LOW = -1e30
+
+PLAN = {
+    0: [],
+    1: [("spread", 0, 1), ("down1", 0)],
+    2: [],
+    3: [("down1", 1)],
+    4: [("ring", 1), ("ring", -1), ("spread", 0, 0), ("spread", 1, 0), ("spread", -1, 1), ("ring", -2), ("spread", -2, 0), ("spread", -1, 0)],
+    5: [("down", 0, 1), ("down1", 2), ("relay", 0, 0), ("spread", 1, 1), ("relay", 1, 0)],
+    6: [("ring", 2), ("up1", 1), ("spread", 2, 0), ("down", 2, 1), ("spread", -2, 1)],
+    7: [("relay", -1, 1), ("spread", 2, 1), ("up", 1, 1)],
+    8: [],
+    9: [("relay", 0, 1), ("down", 1, 1), ("ring", 3), ("down1", 3), ("up1", 3)],
+    10: [("down", 0, 2), ("up", 1, 2)],
+    11: [("up1", 2), ("relay", 2, 1), ("down", 3, 1), ("up", 3, 1), ("ring", -3), ("ring", 4), ("spread", 3, 1), ("up1", 0), ("down", 2, 2), ("spread", -3, 1), ("relay", -2, 1)],
+    12: [("spread", 4, 1), ("down", 3, 2), ("relay", 3, 1), ("up", 0, 1), ("down", 0, 3), ("spread", 3, 0), ("up", 3, 2), ("down", 1, 2), ("up", 2, 1), ("up", 0, 2)],
+    13: [("relay", 4, 1), ("relay", 1, 1), ("relay", -3, 1), ("down", 2, 3), ("down", 1, 3), ("down", 3, 3), ("relay", -1, 0), ("down", 0, 4)],
+    14: [],
+    15: [("up", 2, 2), ("spread", -3, 0), ("up", 1, 3), ("relay", 3, 0)],
+    16: [("relay", -2, 0), ("down", 2, 4)],
+    17: [],
+    18: [],
+    19: [("down", 3, 4), ("relay", 2, 0), ("up", 2, 3), ("up", 3, 3), ("up", 0, 3), ("down", 1, 4)],
+    20: [("spread", 4, 0)],
+    21: [],
+    22: [],
+    23: [("relay", -3, 0)],
+    24: [],
+    25: [("relay", 4, 0)],
+    26: [],
+    27: [],
+}
 
 
 def remote(src, dst, send_sem, recv_sem, device):
@@ -260,16 +291,14 @@
         sems = sems.at[k + w_up]
         return remote(ref, ref, sems.at[0, i], sems.at[1, i], y_peer(side))
 
-    def send_y(k):
-        for rest in (True, False):
-            for side in (1, -1):
-                over_y(rest, k, side).start()
-
-    def pass_y(k):
-        for rest in (True, False):
-            for side in (1, -1):
-                over_y(rest, k, side, True).wait_recv()
-                over_y(rest, k, side, half=True).start()
+    def send_y(rest, k):
+        for side in (1, -1):
+            over_y(rest, k, side).start()
+
+    def pass_y(rest, k):
+        for side in (1, -1):
+            over_y(rest, k, side, True).wait_recv()
+            over_y(rest, k, side, half=True).start()
 
     q_send = y_copies(lambda at: q_all.at[at], q_sem)
     q_arrive = y_copies(lambda at: q_all.at[at], q_sem, True)
@@ -312,6 +341,28 @@
         for copy in copies:
             copy.start()
 
+    def move(kind, k, step=0):
+        if kind == "ring":
+            pass_dnd(k) if k > 0 else pass_dnu(-k)
+        elif kind == "spread":
+            send_y(step == 1, k)
+        elif kind == "relay":
+            pass_y(step == 1, k)
+        elif kind == "down1":
+            if k:
+                upy_arrive[k - 1].wait_recv()
+            upd(k, 1).start()
+        elif kind == "up1":
+            upu(k, 1).start()
+        elif kind == "down":
+            pass_upd(k, step)
+        elif kind == "up":
+            pass_upu(k, step)
+
+    def at(place):
+        for item in PLAN[place]:
+            move(*item)
+
     locals_[0].wait()
     locals_[2].wait()
     start(kv_up_send(0, 1))
@@ -325,9 +376,8 @@
     locals_[5].wait()
     start_all(dnd(1))
     start_all(dnu(1))
-    upd(0, 1).start()
     start_all(upy_send)
-    send_y(0)
+    at(0)
     locals_[6].wait()
     start_all(res_send)
 
@@ -354,6 +404,7 @@
 
     v_ones[:, :hd] = kv_all[z, 1]
     attend(z, y * per_block, per_block, True)
+    at(1)
     for copy in q_arrive:
         copy.wait_recv()
 
@@ -385,43 +436,12 @@
 
         lax.fori_loop(first, last, block, 0)
 
-    forward_kv(1)
-    for d in range(1, ny):
-        upy_arrive[d - 1].wait_recv()
-        upd(d, 1).start()
-    attend_step(1)
-    pass_dnd(1)
-    pass_dnu(1)
-    send_y(1)
-    send_y(-1)
-    pass_y(0)
-
-    forward_kv(2)
-    pass_upd(0, 1)
-    attend_step(2)
-    pass_dnd(2)
-    pass_dnu(2)
-    send_y(2)
-    send_y(-2)
-    pass_y(1)
-
-    forward_kv(3)
-    for d in range(ny):
-        upu(d, 1).start()
-    pass_upd(1, 1)
-    attend_step(3)
-    pass_upd(2, 1)
-    pass_dnd(3)
-    pass_dnu(3)
-    pass_y(-1)
-
-    forward_kv(4)
-    pass_upd(3, 1)
-    pass_upd(0, 2)
-    attend_step(4)
-    pass_upd(1, 2)
-    pass_upd(2, 2)
-    pass_y(2)
+    at(2)
+    for step in range(1, kv_up + 1):
+        forward_kv(step)
+        at(2 * step + 1)
+        attend_step(step)
+        at(2 * step + 2)
 
     eye = lax.broadcasted_iota(jnp.int32, (hd, hd), 0) == lax.broadcasted_iota(jnp.int32, (hd, hd), 1)
 
@@ -437,13 +457,7 @@
     o_recv[y] = o_send[y]
     lse_recv[y] = lse_send[y]
 
-    pass_dnd(4)
-    for k in (3, -3, 4):
-        send_y(k)
-    pass_y(-2)
-    pass_upu(0, 1)
-    pass_upu(1, 1)
-    pass_upd(3, 2)
+    at(11)
 
     for copy in o_copies(True):
         copy.wait_recv()
@@ -463,11 +477,7 @@
         head_copy(d).start()
     head_to_pair(0).start()
 
-    pass_upu(2, 1)
-    pass_upu(3, 1)
-    pass_upd(0, 3)
-    pass_upd(1, 3)
-    pass_y(3)
+    at(12)
 
     locals_[7].wait()
     for copy in res_arrive:
@@ -475,9 +485,7 @@
     for d in range(1, nx):
         head_copy(d, True).wait_recv()
         head_to_pair(d).start()
-    pass_upu(0, 2)
-    pass_upd(2, 3)
-    pass_y(-3)
+    at(13)
     for d in range(nx):
         head_to_pair(d, True).wait_recv()
     n_heads = heads.shape[0]
@@ -494,10 +502,7 @@
     segment = width // COL_TILE // 4
     for i in range(4):
         squares = lax.fori_loop(i * segment, (i + 1) * segment, project, squares)
-        if i < 3:
-            pass_upu(i + 1, 2)
-        else:
-            pass_upd(3, 3)
+        at(14 + i)
     inverse = lax.rsqrt(squares / width + 1e-06)
     top_s[0:tok, :] = jnp.broadcast_to(inverse, (tok, hd))
 
@@ -509,14 +514,12 @@
 
     lax.fori_loop(0, tok // own_rows, normalise, 0)
 
-    pass_y(4)
-
+    at(18)
+
+    at(19)
     for k in range(-w_up, w_down + 1):
         for side in (1, -1):
             over_y(True, k, side, True, True).wait_recv()
-    for d in range(ny):
-        pass_upu(d, 3)
-        pass_upd(d, 4)
     ff = hidden.shape[1]
 
     def up_tile(n, carry):
@@ -561,6 +564,7 @@
             sum_copy(k, d).start()
 
     for i, k in enumerate(order):
+        at(20 + i)
         for side in (1, -1):
             over_y(False, k, side, True, True).wait_recv()
         block = dot(hidden[...], dn_all[wrap(z + k, nz)].reshape(z_cols, ff), ((1,), (1,)))

time: 105 us -> 99.8 us (0.950)
  Pallas kernels: 103 us -> 98 us
    pallas_call x1, Pallas kernels: 103 us -> 98 us  [per_device(): pl.pallas_call(functools.partial(layer_kernel, sizes), out_shape=jax.Shap...]
where the time goes in v3:
time: 99.8 us; the launch traced here: 99.6 us
  Pallas kernels  98 us (98%)
  local copies, waits for them, and re-layouts  1.67 us (2%)
    pallas_call x1, Pallas kernels, per_device(): pl.pallas_call(functools.partial(layer_kernel, sizes), out_shape=jax.Shap...  98 us

profile of v3, /device:TPU:1, one launch (start us, length us, event | category | flops | bytes accessed | tf_op | source)
XLA Modules:
  0.0 99.6 jit_solution(16430270384473261914)
XLA Ops:
  0.0 98.0 %shard_map.91 = bf16[64,2048]{1,0:T(8,128)(2,1)} custom-call(bf16[512,128]{1,0:T(8,128)(2,1)} %q_hbm.1, bf16[512,128]{1,0:T(8,128)(2,1)} %k_hbm.1, bf16[512,128]{1,0:T(8,128)(2,1)} %v_hbm.1, f32[1,512]{1,0:T(1,128)} %bitcast.5, bf16[64,2048]{1,0:T(8,128)(2,1)} %res_hbm.1, bf16[1024,2048]{1,0:T(8,128)(2,1)} %wo_hbm.1, f32[1,2048]{1,0:T(1,128)} %bitcast.4, ...), custom_call_target="tpu_custom_call" | custom-call | tf_op jit(solution)/shard_map/pallas_call | solution.py:621
  98.0 1.7 %copy.11 = bf16[64,2048]{1,0:T(8,128)(2,1)} copy(bf16[64,2048]{1,0:T(8,128)(2,1)} %shard_map.91) | data formatting | bytes 524288

commit v4 on v3

--- a/solution.py
+++ b/solution.py
@@ -35,8 +35,8 @@
     15: [("up", 2, 2), ("spread", -3, 0), ("up", 1, 3), ("relay", 3, 0)],
     16: [("relay", -2, 0), ("down", 2, 4)],
     17: [],
-    18: [],
-    19: [("down", 3, 4), ("relay", 2, 0), ("up", 2, 3), ("up", 3, 3), ("up", 0, 3), ("down", 1, 4)],
+    18: [("relay", 2, 0)],
+    19: [("down", 3, 4), ("up", 2, 3), ("up", 3, 3), ("up", 0, 3), ("down", 1, 4)],
     20: [("spread", 4, 0)],
     21: [],
     22: [],
@@ -516,21 +516,42 @@
 
     at(18)
 
-    at(19)
-    for k in range(-w_up, w_down + 1):
-        for side in (1, -1):
-            over_y(True, k, side, True, True).wait_recv()
+    z_cols = width // nz
     ff = hidden.shape[1]
-
-    def up_tile(n, carry):
+    far = [-w_up, w_down]
+    near = [k for k in range(-w_up, w_down + 1) if k not in far]
+
+    def rest_arrived(levels):
+        for k in levels:
+            for side in (1, -1):
+                over_y(True, k, side, True, True).wait_recv()
+
+    def up_part(levels, cols):
+        total = None
+        for k in levels:
+            slot = wrap(z + k, nz)
+            rows = pl.ds(pl.multiple_of(slot * z_cols, z_cols), z_cols)
+            term = dot(normed[:, rows], up_all[slot, :, :, cols].reshape(z_cols, COL_TILE))
+            total = term if total is None else total + term
+        return total
+
+    def near_tile(n, carry):
         cols = pl.ds(pl.multiple_of(n * COL_TILE, COL_TILE), COL_TILE)
-        proj = dot(normed[...], up_all[:, :, :, cols].reshape(width, COL_TILE))
+        acc_s[pl.ds(pl.multiple_of(n * tok, tok), tok), :] = up_part(near, cols)
+        return carry
+
+    def far_tile(n, carry):
+        cols = pl.ds(pl.multiple_of(n * COL_TILE, COL_TILE), COL_TILE)
+        proj = acc_s[pl.ds(pl.multiple_of(n * tok, tok), tok), :] + up_part(far, cols)
         hidden[:, cols] = jnp.square(jnp.maximum(proj, 0.0)).astype(jnp.bfloat16)
         return carry
 
-    lax.fori_loop(0, ff // COL_TILE, up_tile, 0)
-
-    z_cols = width // nz
+    rest_arrived(near)
+    lax.fori_loop(0, ff // COL_TILE, near_tile, 0)
+    at(19)
+    rest_arrived(far)
+    lax.fori_loop(0, ff // COL_TILE, far_tile, 0)
+
     order = [0] + [s for k in range(1, w_up + 1) for s in (k, -k)] + list(range(w_up + 1, w_down + 1))
 
     def cols_of(k):

time: 99.8 us -> 100 us (level)
  no operation moved by 1% of the time
where the time goes in v4:
time: 100 us
  Pallas kernels  98.3 us (98%)
  local copies, waits for them, and re-layouts  1.67 us (2%)
    pallas_call x1, Pallas kernels, per_device(): pl.pallas_call(functools.partial(layer_kernel, sizes), out_shape=jax.Shap...  98.3 us

profile of v4, /device:TPU:1, one launch (start us, length us, event | category | flops | bytes accessed | tf_op | source)
XLA Modules:
  0.0 100.0 jit_solution(9790294827997581416)
XLA Ops:
  0.0 98.3 %shard_map.91 = bf16[64,2048]{1,0:T(8,128)(2,1)} custom-call(bf16[512,128]{1,0:T(8,128)(2,1)} %q_hbm.1, bf16[512,128]{1,0:T(8,128)(2,1)} %k_hbm.1, bf16[512,128]{1,0:T(8,128)(2,1)} %v_hbm.1, f32[1,512]{1,0:T(1,128)} %bitcast.5, bf16[64,2048]{1,0:T(8,128)(2,1)} %res_hbm.1, bf16[1024,2048]{1,0:T(8,128)(2,1)} %wo_hbm.1, f32[1,2048]{1,0:T(1,128)} %bitcast.4, ...), custom_call_target="tpu_custom_call" | custom-call | tf_op jit(solution)/shard_map/pallas_call | solution.py:642
  98.3 1.7 %copy.11 = bf16[64,2048]{1,0:T(8,128)(2,1)} copy(bf16[64,2048]{1,0:T(8,128)(2,1)} %shard_map.91) | data formatting | bytes 524288
